TPU v7x, 512 devices: a whole 4x8x8 slice. The times are simulated.
512 devices in a mesh: ep: 32 (over z, x), tp: 16 (over y, core).
Axes of the slice: x: 4, y: 8, z: 8, core: 2. Of those that a mesh axis runs over, the one named last changes fastest.
Arguments:
- query_rows: bfloat16 [16384, 3072], P('ep', 'tp'), may hold values from -6 to 6
- key_rows: bfloat16 [16384, 1024], P('ep', 'tp'), may hold values from -6 to 6
- value_rows: bfloat16 [16384, 1024], P('ep', 'tp'), may hold values from -6 to 6
- query_gain: float32 [48, 64], P('tp'), may hold values from 0.4 to 48
- key_gain: float32 [16, 64], P('tp'), may hold values from 0.1 to 1.9
- sink_logits: float32 [48], P('tp'), may hold values from 1 to 6
- out_weight: bfloat16 [3072, 2048], P('tp'), may hold values from -0.109375 to 0.109375
- expert_input: bfloat16 [16384, 2048], P(('ep', 'tp')), may hold values from -6 to 6
- expert_gain: float32 [2048], replicated, may hold values from 0.1 to 1.9
- routes: int32 [16384, 2], P(('ep', 'tp')), may hold values from 0 to 31, all different within a row; in each aligned block of 32 rows (0 to 31, 32 to 63, ...) at most 3 rows name the same one
- route_logits: float32 [16384, 2], P(('ep', 'tp')), may hold values from -6 to 6
- gate_weight: bfloat16 [32, 2048, 2048], P('ep', None, 'tp'), may hold values from -0.375 to 0.375
- up_weight: bfloat16 [32, 2048, 2048], P('ep', None, 'tp'), may hold values from -0.375 to 0.375
- down_weight: bfloat16 [32, 2048, 2048], P('ep', 'tp'), may hold values from -0.01953125 to 0.01953125
Outputs:
- attended: bfloat16 [16384, 2048], P(('ep', 'tp'))
- expert_mix: bfloat16 [16384, 2048], P(('ep', 'tp'))
Inputs may be any that keep to these rules, and one draw needn't show every extreme that they name: `routes`: each row names 2 different experts; in the rows of one device no expert is named more than 3 times, and in some device one expert is named exactly 3 times.
All inputs are finite; a program needn't handle non-finite values.
Results may differ from a plain program's by a relative error of at most 0.017.
The roundings to bfloat16 on the way count: a program that leaves them out, or rounds other values in their place, can miss the bound.
Values may be sent and summed in bfloat16 or wider, within the bound.
A program may use at most 64 MiB of HBM per device.

v0:
```python
import jax
import jax.numpy as jnp
from jax import lax
from jax.sharding import PartitionSpec as P

EXPERTS = 32
WINDOW = 128
EPSILON = 1e-06
CLAMP_LIMIT = 7.0
ACT_SLOPE = 1.702
NEGATIVE = -1e30


def shifted(value, axis, steps):
    count = lax.axis_size(axis)
    initial, last = (max(0, -steps), min(count, count - steps))
    return lax.ppermute(value, axis, [(source, source + steps) for source in range(initial, last)])


def head_norm(row_data, gain_table):
    head_count, head_size = gain_table.shape
    widened = row_data.astype(jnp.float32).reshape(row_data.shape[0], head_count, head_size)
    scaled = widened * lax.rsqrt(jnp.mean(widened * widened, axis=-1, keepdims=True) + EPSILON)
    return (scaled * gain_table).astype(jnp.bfloat16)


def band(padded, blocks):
    tiled = padded.reshape((blocks + 1, WINDOW) + padded.shape[1:])
    return jnp.concatenate([tiled[:-1], tiled[1:]], axis=1)


def attend(query_rows, key_rows, value_rows, query_gain, key_gain, sink_logits):
    seq_rows = query_rows.shape[0]
    key_heads, head_size = key_gain.shape
    group_size = query_gain.shape[0] // key_heads
    blocks = seq_rows // WINDOW
    query_hat = head_norm(query_rows, query_gain).reshape(
        blocks, WINDOW, key_heads, group_size, head_size
    )
    key_hat = head_norm(key_rows, key_gain)
    value_hat = value_rows.reshape(seq_rows, key_heads, head_size)
    tail_rows = jnp.stack([key_hat[seq_rows - WINDOW :], value_hat[seq_rows - WINDOW :]])
    earlier = shifted(tail_rows, "ep", 1)
    key_band = band(jnp.concatenate([earlier[0], key_hat], axis=0), blocks)
    value_band = band(jnp.concatenate([earlier[1], value_hat], axis=0), blocks)
    query_pos = lax.broadcasted_iota(jnp.int32, (WINDOW, 2 * WINDOW), 0)
    key_pos = lax.broadcasted_iota(jnp.int32, (WINDOW, 2 * WINDOW), 1)
    distance = query_pos + WINDOW - key_pos
    inside = (distance >= 0) & (distance < WINDOW)
    first_block = (lax.broadcasted_iota(jnp.int32, (blocks, 1, 1), 0) == 0) & (
        lax.axis_index("ep") == 0
    )
    allowed = inside[None] & ~(first_block & (key_pos < WINDOW)[None])
    scores = jnp.einsum(
        "bqkgd,bjkd->bkgqj", query_hat, key_band, preferred_element_type=jnp.float32
    ) * head_size ** (-0.5)
    scores = jnp.where(allowed[:, None, None], scores, NEGATIVE)
    sink_table = sink_logits.reshape(1, key_heads, group_size, 1, 1)
    highest = jnp.maximum(jnp.max(scores, axis=-1, keepdims=True), sink_table)
    weights = jnp.exp(scores - highest)
    total = jnp.sum(weights, axis=-1, keepdims=True) + jnp.exp(sink_table - highest)
    mixed = jnp.einsum(
        "bkgqj,bjkd->bkgqd",
        weights.astype(jnp.bfloat16),
        value_band,
        preferred_element_type=jnp.float32,
    )
    mixed = (mixed / total).astype(jnp.bfloat16)
    return jnp.transpose(mixed, (0, 3, 1, 2, 4)).reshape(seq_rows, -1)


def slot_maps(route_block, capacity):
    flat_routes = route_block.reshape(-1)
    expert_hot = (flat_routes[:, None] == lax.broadcasted_iota(jnp.int32, (1, EXPERTS), 1)).astype(
        jnp.int32
    )
    before = jnp.cumsum(expert_hot, axis=0) - expert_hot
    position = jnp.sum(before * expert_hot, axis=1)
    place_hot = (position[:, None] == lax.broadcasted_iota(jnp.int32, (1, capacity), 1)).astype(
        jnp.float32
    )
    row_total, fanout = route_block.shape
    return (
        expert_hot.astype(jnp.float32).reshape(row_total, fanout, EXPERTS),
        place_hot.reshape(row_total, fanout, capacity),
    )


def dispatch_matrix(route_block, capacity):
    expert_hot, place_hot = slot_maps(route_block, capacity)
    return jnp.einsum("rke,rkc->ecr", expert_hot, place_hot).astype(jnp.bfloat16)


def combine_matrix(route_block, route_weight, capacity):
    expert_hot, place_hot = slot_maps(route_block, capacity)
    return jnp.einsum("rke,rkc,rk->rec", expert_hot, place_hot, route_weight)


def expert_hidden(piece, gate_weight, up_weight):
    gate_pre = jnp.einsum("aecd,edf->aecf", piece, gate_weight, preferred_element_type=jnp.float32)
    up_pre = jnp.einsum("aecd,edf->aecf", piece, up_weight, preferred_element_type=jnp.float32)
    clipped = jnp.minimum(gate_pre, CLAMP_LIMIT)
    linear = jnp.clip(up_pre, -CLAMP_LIMIT, CLAMP_LIMIT)
    return (clipped * jax.nn.sigmoid(ACT_SLOPE * clipped) * (linear + 1.0)).astype(jnp.bfloat16)


def on_device(
    query_rows,
    key_rows,
    value_rows,
    query_gain,
    key_gain,
    sink_logits,
    out_weight,
    expert_input,
    expert_gain,
    routes,
    route_logits,
    gate_weight,
    up_weight,
    down_weight,
):
    heads_out = attend(query_rows, key_rows, value_rows, query_gain, key_gain, sink_logits)
    attended = lax.psum_scatter(
        jnp.dot(heads_out, out_weight, preferred_element_type=jnp.float32).astype(jnp.bfloat16),
        "tp",
        scatter_dimension=0,
        tiled=True,
    )
    own_rows = expert_input.shape[0]
    fanout = routes.shape[1]
    capacity = (3 * own_rows * fanout + 2 * EXPERTS - 1) // (2 * EXPERTS)
    ep_size = lax.axis_size("ep")
    tp_size = lax.axis_size("tp")
    local_experts = gate_weight.shape[0]
    widened = expert_input.astype(jnp.float32)
    normed = (
        widened
        * lax.rsqrt(jnp.mean(widened * widened, axis=-1, keepdims=True) + EPSILON)
        * expert_gain
    ).astype(jnp.bfloat16)
    route_weight = jax.nn.softmax(route_logits, axis=-1)
    combine = combine_matrix(routes, route_weight, capacity)
    sender = dispatch_matrix(routes, capacity)
    slot_rows = jnp.einsum(
        "ecr,rd->ecd", sender, normed, preferred_element_type=jnp.float32
    ).astype(jnp.bfloat16)
    slot_rows = slot_rows.reshape(ep_size, local_experts, capacity, -1)
    arrived = lax.all_to_all(slot_rows, "ep", split_axis=0, concat_axis=0, tiled=True)
    hidden_units = expert_hidden(
        lax.all_gather(arrived, "tp", axis=0, tiled=True), gate_weight, up_weight
    )
    partial_value = jnp.einsum(
        "aecf,efd->aecd", hidden_units, down_weight, preferred_element_type=jnp.float32
    ).astype(jnp.bfloat16)
    partial_value = partial_value.reshape(tp_size, ep_size * local_experts * capacity, -1)
    pieces = lax.all_to_all(partial_value, "tp", split_axis=0, concat_axis=0, tiled=True)
    summed = jnp.sum(pieces, axis=0, dtype=jnp.float32).astype(jnp.bfloat16)
    summed = summed.reshape(ep_size, local_experts * capacity, -1)
    returned = lax.all_to_all(summed, "ep", split_axis=0, concat_axis=0, tiled=True)
    expert_mix = jnp.einsum("rec,ecd->rd", combine, returned.astype(jnp.float32)).astype(
        jnp.bfloat16
    )
    return (attended, expert_mix)


def solution(mesh):
    placed = (
        P("ep", "tp"),
        P("ep", "tp"),
        P("ep", "tp"),
        P("tp", None),
        P("tp", None),
        P("tp"),
        P("tp", None),
        P(("ep", "tp"), None),
        P(),
        P(("ep", "tp"), None),
        P(("ep", "tp"), None),
        P("ep", None, "tp"),
        P("ep", None, "tp"),
        P("ep", "tp", None),
    )
    return jax.shard_map(
        on_device,
        mesh=mesh,
        in_specs=placed,
        out_specs=(P(("ep", "tp"), None), P(("ep", "tp"), None)),
        check_vma=False,
    )
```

profile of v0, /device:TPU:24, one launch (start us, length us, event | category | flops | bytes accessed | tf_op | source)
XLA Modules:
  0.0 328.0 jit_solution(9556012948772609825)
XLA Ops:
  7.2 1.1 fusion.58
  8.3 0.8 copy.42
  9.4 0.2 select_reduce_fusion
  9.6 0.1 eq.72
  9.7 0.4 fusion.34
  10.1 1.2 fusion.4
  11.3 0.3 copy.46
  11.6 30.7 %all_to_all.15 = bf16[32,1,3,2048]{3,2,1,0:T(4,128)(2,1)S(1)} all-to-all(bf16[32,1,3,2048]{3,2,1,0:T(4,128)(2,1)S(1)} %copy.46), channel_id=1, replica_groups=mesh['ep'=32,'tp'=16] {'ep'}, dimensions={0} | all-to-all | bytes 786432 | tf_op jit(solution)/shard_map/all_to_all | solution.py:149
  42.3 1.1 copy.47
  43.5 44.1 %all-gather.2.cloned.1.call-done = bf16[512,1,3,2048]{3,0,2,1:T(8,128)(2,1)} async-done(((bf16[32,1,3,2048]{3,0,2,1:T(8,128)(2,1)}), bf16[512,1,3,2048]{3,0,2,1:T(8,128)(2,1)}) %all-gather.2.cloned.1.call-update) | async-done | bytes 6291472 | tf_op jit(solution)/shard_map/all_gather | solution.py:151
  87.5 4.6 %fusion.11 = f32[512,1,3,128]{3,0,2,1:T(8,128)S(1)} fusion(bf16[512,1,3,2048]{3,0,2,1:T(8,128)(2,1)} %all-gather.2.cloned.1.call-done, bf16[1,2048,128]{2,1,0:T(8,128)(2,1)S(1)} %copy-done.9), kind=kOutput, calls=%fused_computation.15 | convolution fusion | flops 805502976 | bytes 7602176 | tf_op jit(solution)/shard_map/aecd,edf->aecf/dot_general | solution.py:100
  92.1 11.9 %convert_bitcast_fusion = bf16[512,1,3,2048]{3,0,2,1:T(8,128)(2,1)} fusion(bf16[512,1,3,2048]{3,0,2,1:T(8,128)(2,1)} %all-gather.2.cloned.1.call-done, f32[512,1,3,128]{3,0,2,1:T(8,128)S(1)} %fusion.11, bf16[1,128,2048]{2,1,0:T(8,128)(2,1)S(1)} %copy-done.3, bf16[1,2048,128]{2,1,0:T(8,128)(2,1)S(1)} %copy-done.4), kind=kOutput, calls=%fused_computation.4 | convolution fusion | flops 1615527936 | bytes 14417920 | tf_op jit(solution)/shard_map/aecf,efd->aecd/dot_general | solution.py:153
  104.1 11.6 %copy.48 = bf16[512,1,3,2048]{3,2,0,1:T(4,128)(2,1)} copy(bf16[512,1,3,2048]{3,0,2,1:T(8,128)(2,1)} %convert_bitcast_fusion) | data formatting | bytes 12582912 | tf_op jit(solution)/shard_map/convert_element_type | solution.py:155
  115.6 16.3 %reshape.224 = bf16[16,96,2048]{2,1,0:T(8,128)(2,1)} reshape(bf16[512,1,3,2048]{3,2,0,1:T(4,128)(2,1)} %copy.48) | data formatting | bytes 12582912 | tf_op jit(solution)/shard_map/reshape | solution.py:156
  132.0 5.5 %all-to-all-start.1 = ((bf16[16,96,2048]{2,1,0:T(8,128)(2,1)}), bf16[16,96,2048]{2,1,0:T(8,128)(2,1)}, u32[]{:S(2)}, u32[]{:S(2)}) async-start(bf16[16,96,2048]{2,1,0:T(8,128)(2,1)} %reshape.224), calls=%async_computation.2 | async-start | bytes 12582912 | tf_op jit(solution)/shard_map/all_to_all | solution.py:157
  137.7 3.4 %collective-permute-start = (bf16[2,128,1,64]{1,3,2,0:T(8,128)(2,1)S(1)}, bf16[2,128,1,64]{1,3,2,0:T(8,128)(2,1)S(1)}, u32[]{:S(2)}, u32[]{:S(2)}) collective-permute-start(bf16[2,128,1,64]{1,3,2,0:T(8,128)(2,1)S(1)} %pad_maximum_fusion.2), channel_id=1, source_target_pairs={{0,16},{16,32},{32,48},{48,64},{64,80},{80,96},{96,112},{112,128},... | collective-permute-start | bytes 98312 | tf_op jit(solution)/shard_map/ppermute | solution.py:17
  141.4 0.2 not_and_fusion
  141.6 0.1 reshape.213
  141.8 0.9 collective-permute-done
  142.7 0.5 fusion.105
  143.3 0.2 fusion.6
  143.6 0.4 fusion.33
  144.0 0.2 copy.41
  144.1 2.1 convolution_convert_fusion
  146.3 140.4 %all-to-all-done.1 = bf16[16,96,2048]{2,1,0:T(8,128)(2,1)} async-done(((bf16[16,96,2048]{2,1,0:T(8,128)(2,1)}), bf16[16,96,2048]{2,1,0:T(8,128)(2,1)}, u32[]{:S(2)}, u32[]{:S(2)}) %all-to-all-start.1) | async-done | bytes 6291488 | tf_op jit(solution)/shard_map/all_to_all | solution.py:157
  286.7 4.1 %reduce_sum.76 = bf16[96,2048]{1,0:T(8,128)(2,1)S(1)} reduce(bf16[16,96,2048]{2,1,0:T(8,128)(2,1)} %all-to-all-done.1, bf16[]{:T(256)} %constant.49.clone.1), dimensions={0}, to_apply=%region_10.11 | reduce | flops 2949120 | bytes 6684674 | tf_op jit(solution)/shard_map/reduce_sum | solution.py:158
  290.8 1.0 reshape.225
  291.8 10.2 %all-to-all-start.2 = ((bf16[32,3,2048]{2,1,0:T(4,128)(2,1)}), bf16[32,3,2048]{2,1,0:T(4,128)(2,1)S(1)}, u32[]{:S(2)}, u32[]{:S(2)}) async-start(bf16[32,3,2048]{2,1,0:T(4,128)(2,1)} %reshape.225), calls=%async_computation.3 | async-start | bytes 1048576 | tf_op jit(solution)/shard_map/all_to_all | solution.py:160
  302.0 0.1 copy.44
  302.2 0.4 fusion.84
  302.5 17.5 %all-to-all-done.2 = bf16[32,3,2048]{2,1,0:T(4,128)(2,1)S(1)} async-done(((bf16[32,3,2048]{2,1,0:T(4,128)(2,1)}), bf16[32,3,2048]{2,1,0:T(4,128)(2,1)S(1)}, u32[]{:S(2)}, u32[]{:S(2)}) %all-to-all-start.2) | async-done | bytes 393248 | tf_op jit(solution)/shard_map/all_to_all | solution.py:160
  320.1 1.1 fusion.5
  (56 shorter events, 1.1 us)
Async XLA Ops:
  7.2 137.0 %copy-start = (bf16[192,2048]{1,0:T(8,128)(2,1)S(1)}, bf16[192,2048]{1,0:T(8,128)(2,1)}, u32[]{:S(2)}) copy-start(bf16[192,2048]{1,0:T(8,128)(2,1)} %param.20) | copy-start | bytes 2359300
  7.2 80.4 %all-gather.2.cloned.1.call-start = ((), (), s32[]{:S(2)}) async-start(), calls=%async_computation.5 | async-start | bytes 6684672 | tf_op jit(solution)/shard_map/all_gather | solution.py:151
  9.7 77.9 %copy-start.9 = (bf16[1,2048,128]{2,1,0:T(8,128)(2,1)S(1)}, bf16[1,2048,128]{2,1,0:T(8,128)(2,1)}, u32[]{:S(2)}) copy-start(bf16[1,2048,128]{2,1,0:T(8,128)(2,1)} %param.25) | copy-start | bytes 1572868
  43.4 48.7 %copy-start.3 = (bf16[1,128,2048]{2,1,0:T(8,128)(2,1)S(1)}, bf16[1,128,2048]{2,1,0:T(8,128)(2,1)}, u32[]{:S(2)}) copy-start(bf16[1,128,2048]{2,1,0:T(8,128)(2,1)} %param.27) | copy-start | bytes 1572868
  43.4 48.7 %copy-start.4 = (bf16[1,2048,128]{2,1,0:T(8,128)(2,1)S(1)}, bf16[1,2048,128]{2,1,0:T(8,128)(2,1)}, u32[]{:S(2)}) copy-start(bf16[1,2048,128]{2,1,0:T(8,128)(2,1)} %param.26) | copy-start | bytes 1572868
  131.9 5.6 %copy-start.2 = (bf16[512,64]{0,1:T(8,128)(2,1)S(1)}, bf16[512,64]{0,1:T(8,128)(2,1)}, u32[]{:S(2)}) copy-start(bf16[512,64]{0,1:T(8,128)(2,1)} %param.15) | copy-start | bytes 196612
  132.0 5.6 %copy-start.7 = (f32[1,64]{1,0:T(1,128)S(1)}, f32[1,64]{1,0:T(1,128)}, u32[]{:S(2)}) copy-start(f32[1,64]{1,0:T(1,128)} %param.18) | copy-start | bytes 772
  132.0 5.7 %copy-start.5 = (bf16[512,64]{0,1:T(8,128)(2,1)S(1)}, bf16[512,64]{0,1:T(8,128)(2,1)}, u32[]{:S(2)}) copy-start(bf16[512,64]{0,1:T(8,128)(2,1)} %param.16) | copy-start | bytes 196612
  132.0 9.1 %copy-start.1 = (bf16[512,192]{0,1:T(8,128)(2,1)S(1)}, bf16[512,192]{0,1:T(8,128)(2,1)}, u32[]{:S(2)}) copy-start(bf16[512,192]{0,1:T(8,128)(2,1)} %param.14) | copy-start | bytes 589828
  132.0 154.7 %all-to-all-start.1 = ((bf16[16,96,2048]{2,1,0:T(8,128)(2,1)}), bf16[16,96,2048]{2,1,0:T(8,128)(2,1)}, u32[]{:S(2)}, u32[]{:S(2)}) async-start(bf16[16,96,2048]{2,1,0:T(8,128)(2,1)} %reshape.224), calls=%async_computation.2 | async-start | bytes 12582912 | tf_op jit(solution)/shard_map/all_to_all | solution.py:157
  137.5 5.3 %copy-start.10 = (f32[3,64]{1,0:T(4,128)S(1)}, f32[3,64]{1,0:T(4,128)}, u32[]{:S(2)}) copy-start(f32[3,64]{1,0:T(4,128)} %param.17) | copy-start | bytes 2308
  137.5 183.7 %reduce-scatter.2.cloned.1.call-start = ((), (), s32[]{:S(2)}) async-start(), calls=%async_computation.4 | async-start | bytes 2228224 | tf_op jit(solution)/shard_map/reduce_scatter | solution.py:124
  137.7 5.0 %collective-permute-start = (bf16[2,128,1,64]{1,3,2,0:T(8,128)(2,1)S(1)}, bf16[2,128,1,64]{1,3,2,0:T(8,128)(2,1)S(1)}, u32[]{:S(2)}, u32[]{:S(2)}) collective-permute-start(bf16[2,128,1,64]{1,3,2,0:T(8,128)(2,1)S(1)} %pad_maximum_fusion.2), channel_id=1, source_target_pairs={{0,16},{16,32},{32,48},{48,64},{64,80},{80,96},{96,112},{112,128},... | collective-permute-start | bytes 98312 | tf_op jit(solution)/shard_map/ppermute | solution.py:17
  141.2 2.0 copy-start.8
  146.3 155.7 %copy-start.6 = (f32[32,2]{0,1:T(2,128)S(1)}, f32[32,2]{0,1:T(2,128)}, u32[]{:S(2)}) copy-start(f32[32,2]{0,1:T(2,128)} %param.24) | copy-start | bytes 772
  291.8 28.3 %all-to-all-start.2 = ((bf16[32,3,2048]{2,1,0:T(4,128)(2,1)}), bf16[32,3,2048]{2,1,0:T(4,128)(2,1)S(1)}, u32[]{:S(2)}, u32[]{:S(2)}) async-start(bf16[32,3,2048]{2,1,0:T(4,128)(2,1)} %reshape.225), calls=%async_computation.3 | async-start | bytes 1048576 | tf_op jit(solution)/shard_map/all_to_all | solution.py:160
Sparse Core Ops, SparseCore 0:
  43.6 43.9 all-gather.1
  146.4 136.6 reduce-scatter.1
where the time goes:
time: 329 us; the launch traced here: 328 us
  waiting for transfers between devices  203 us (62%)
  local copies, waits for them, and re-layouts  31.8 us (10%)
  blocking collectives  30.7 us (9%)
  matrix products  22.5 us (7%)
  starting transfers between devices  19.1 us (6%)
  between operations  14.4 us (4%)
  other arithmetic  6.53 us (2%)
    all_to_all x1, waiting for transfers between devices, on_device(): lax.all_to_all(partial_value, 'tp', split_axis=0, concat_axis=0, tiled=True)  140 us
    all_gather x1, waiting for transfers between devices, on_device(): lax.all_gather(arrived, 'tp', axis=0, tiled=True)  44.1 us
    all_to_all x1, blocking collectives, on_device(): lax.all_to_all(slot_rows, 'ep', split_axis=0, concat_axis=0, tiled=True)  30.7 us
    all_to_all x1, waiting for transfers between devices, on_device(): lax.all_to_all(summed, 'ep', split_axis=0, concat_axis=0, tiled=True)  17.5 us
    reshape x1, local copies, waits for them, and re-layouts, on_device(): partial_value.reshape(tp_size, ep_size * local_experts * capacity, -1)  16.3 us
    dot_general x1, matrix products, on_device(): jnp.einsum('aecf,efd->aecd', hidden_units, down_weight, preferred_element...  11.9 us
    convert_element_type x1, local copies, waits for them, and re-layouts, on_device(): partial_value = jnp.einsum('aecf,efd->aecd', hidden_units, down_weight, p...  11.6 us
    all_to_all x1, starting transfers between devices, on_device(): lax.all_to_all(summed, 'ep', split_axis=0, concat_axis=0, tiled=True)  10.2 us
  transfers between devices with their start and end apart: 5, of which 4 were waited for; matrix products, arithmetic and copies ran while one was open for 3% of the time, Pallas kernels for 0%

commit v1 on v0

--- a/solution.py
+++ b/solution.py
@@ -1,3 +1,4 @@
+import functools
 import jax
 import jax.numpy as jnp
 from jax import lax
@@ -9,6 +10,36 @@
 CLAMP_LIMIT = 7.0
 ACT_SLOPE = 1.702
 NEGATIVE = -1e30
+
+
+def sheets_spread(local, lane_axis, d_out):
+    g_now = jax.lax.axis_size(lane_axis)
+    plain = jax.lax.axis_index(lane_axis)
+    v_now, everything, answer = (g_now, plain, local.shape[d_out])
+    all_rows = tuple(((s, (s + 1) % v_now) for s in range(v_now)))
+    rows = tuple(((s, (s - 1) % v_now) for s in range(v_now)))
+    far_arr = jnp.zeros(
+        (*local.shape[:d_out], v_now * answer, *local.shape[d_out + 1 :]), local.dtype
+    )
+    far_arr = lax.dynamic_update_slice_in_dim(far_arr, local, everything * answer, axis=d_out)
+    m_next = found_now = local
+    long_array = v_now // 2
+    kk = 1
+    while kk < long_array + 1:
+        m_next = jax.lax.ppermute(m_next, lane_axis, all_rows)
+        far_arr = lax.dynamic_update_slice_in_dim(
+            far_arr, m_next, (everything - kk) % v_now * answer, axis=d_out
+        )
+        if kk < v_now - long_array:
+            found_now = jax.lax.ppermute(found_now, lane_axis, rows)
+            far_arr = lax.dynamic_update_slice_in_dim(
+                far_arr, found_now, (everything + kk) % v_now * answer, axis=d_out
+            )
+        kk += 1
+    return far_arr
+
+
+shape_the_columns = functools.partial(sheets_spread, lane_axis="tp", d_out=0)
 
 
 def shifted(value, axis, steps):
@@ -147,9 +178,7 @@
     ).astype(jnp.bfloat16)
     slot_rows = slot_rows.reshape(ep_size, local_experts, capacity, -1)
     arrived = lax.all_to_all(slot_rows, "ep", split_axis=0, concat_axis=0, tiled=True)
-    hidden_units = expert_hidden(
-        lax.all_gather(arrived, "tp", axis=0, tiled=True), gate_weight, up_weight
-    )
+    hidden_units = expert_hidden(shape_the_columns(arrived), gate_weight, up_weight)
     partial_value = jnp.einsum(
         "aecf,efd->aecd", hidden_units, down_weight, preferred_element_type=jnp.float32
     ).astype(jnp.bfloat16)

time: 329 us -> 360 us (1.094)
  starting transfers between devices: 19.1 us -> 68.8 us
  blocking collectives: 30.7 us -> 0 us
  local copies, waits for them, and re-layouts: 31.8 us -> 39.9 us
  waiting for transfers between devices: 203 us -> 209 us
    all_gather x1 -> x0, waiting for transfers between devices: 44.1 us -> none  [on_device(): lax.all_gather(arrived, 'tp', axis=0, tiled=True)]
    ppermute x0 -> x15, waiting for transfers between devices: none -> 32.1 us  [the longest x8 32.1 us: sheets_spread(): m_next = jax.lax.ppermute(m_next, lane_axis, all_rows)]
    ppermute x0 -> x15, starting transfers between devices: none -> 31.7 us  [the longest x8 28.4 us: sheets_spread(): m_next = jax.lax.ppermute(m_next, lane_axis, all_rows)]
    all_to_all x1 -> x0, blocking collectives: 30.7 us -> none  [on_device(): lax.all_to_all(slot_rows, 'ep', split_axis=0, concat_axis=0, tiled=True)]
    all_to_all x0 -> x1, waiting for transfers between devices: none -> 17.5 us  [on_device(): lax.all_to_all(slot_rows, 'ep', split_axis=0, concat_axis=0, tiled=True)]
    all_to_all x0 -> x1, starting transfers between devices: none -> 13.2 us  [on_device(): lax.all_to_all(slot_rows, 'ep', split_axis=0, concat_axis=0, tiled=True)]
    all_to_all x1, starting transfers between devices: 5.5 us -> 16.5 us  [on_device(): lax.all_to_all(partial_value, 'tp', split_axis=0, concat_axis=0, tiled=True)]
    all_to_all x1, starting transfers between devices: 10.2 us -> 4.64 us  [on_device(): lax.all_to_all(summed, 'ep', split_axis=0, concat_axis=0, tiled=True)]
  transfers between devices with their start and end apart: 5 -> 20, of which waited for: 4 -> 12; matrix products, arithmetic and copies ran while one was open for 3% -> 5% of each run, Pallas kernels for 0% -> 0%
where the time goes in v1:
time: 360 us; the launch traced here: 359 us
  waiting for transfers between devices  209 us (58%)
  starting transfers between devices  68.8 us (19%)
  local copies, waits for them, and re-layouts  39.9 us (11%)
  matrix products  19.9 us (6%)
  between operations  14.9 us (4%)
  other arithmetic  6.46 us (2%)
    all_to_all x1, waiting for transfers between devices, on_device(): lax.all_to_all(partial_value, 'tp', split_axis=0, concat_axis=0, tiled=True)  141 us
    ppermute x8, waiting for transfers between devices, sheets_spread(): m_next = jax.lax.ppermute(m_next, lane_axis, all_rows)  32.1 us
    ppermute x8, starting transfers between devices, sheets_spread(): m_next = jax.lax.ppermute(m_next, lane_axis, all_rows)  28.4 us
    all_to_all x1, waiting for transfers between devices, on_device(): lax.all_to_all(summed, 'ep', split_axis=0, concat_axis=0, tiled=True)  17.5 us
    all_to_all x1, waiting for transfers between devices, on_device(): lax.all_to_all(slot_rows, 'ep', split_axis=0, concat_axis=0, tiled=True)  17.5 us
    all_to_all x1, starting transfers between devices, on_device(): lax.all_to_all(partial_value, 'tp', split_axis=0, concat_axis=0, tiled=True)  16.5 us
    reshape x1, local copies, waits for them, and re-layouts, on_device(): partial_value.reshape(tp_size, ep_size * local_experts * capacity, -1)  16.3 us
    all_to_all x1, starting transfers between devices, on_device(): lax.all_to_all(slot_rows, 'ep', split_axis=0, concat_axis=0, tiled=True)  13.2 us
  transfers between devices with their start and end apart: 20, of which 12 were waited for; matrix products, arithmetic and copies ran while one was open for 5% of the time, Pallas kernels for 0%

profile of v1, /device:TPU:24, one launch (start us, length us, event | category | flops | bytes accessed | tf_op | source)
XLA Modules:
  0.0 359.0 jit_solution(12004405431145661923)
XLA Ops:
  10.0 1.2 fusion
  11.2 1.1 copy.46
  12.4 13.2 %all-to-all-start = ((bf16[32,1,3,2048]{3,2,1,0:T(4,128)(2,1)}), bf16[32,1,3,2048]{3,2,1,0:T(4,128)(2,1)S(1)}, u32[]{:S(2)}, u32[]{:S(2)}) async-start(bf16[32,1,3,2048]{3,2,1,0:T(4,128)(2,1)} %copy.46), calls=%async_computation.1 | async-start | bytes 1048576 | tf_op jit(solution)/shard_map/all_to_all | solution.py:180
  25.8 17.5 %all-to-all-done = bf16[32,1,3,2048]{3,2,1,0:T(4,128)(2,1)S(1)} async-done(((bf16[32,1,3,2048]{3,2,1,0:T(4,128)(2,1)}), bf16[32,1,3,2048]{3,2,1,0:T(4,128)(2,1)S(1)}, u32[]{:S(2)}, u32[]{:S(2)}) %all-to-all-start) | async-done | bytes 393248 | tf_op jit(solution)/shard_map/all_to_all | solution.py:180
  43.3 1.7 collective-permute-start.2
  46.2 5.8 %collective-permute-done.1 = bf16[32,1,3,2048]{3,2,1,0:T(4,128)(2,1)S(1)} collective-permute-done((bf16[32,1,3,2048]{3,2,1,0:T(4,128)(2,1)S(1)}, bf16[32,1,3,2048]{3,2,1,0:T(4,128)(2,1)S(1)}, u32[]{:S(2)}, u32[]{:S(2)}) %collective-permute-start.1) | collective-permute-done | bytes 393248 | tf_op jit(solution)/shard_map/ppermute | solution.py:29
  52.7 1.3 collective-permute-start.4
  54.3 6.2 %collective-permute-done.3 = bf16[32,1,3,2048]{3,2,1,0:T(4,128)(2,1)S(1)} collective-permute-done((bf16[32,1,3,2048]{3,2,1,0:T(4,128)(2,1)S(1)}, bf16[32,1,3,2048]{3,2,1,0:T(4,128)(2,1)S(1)}, u32[]{:S(2)}, u32[]{:S(2)}) %collective-permute-start.3) | collective-permute-done | bytes 393248 | tf_op jit(solution)/shard_map/ppermute | solution.py:29
  60.5 1.6 collective-permute-start.5
  62.9 6.2 %collective-permute-done.5 = bf16[32,1,3,2048]{3,2,1,0:T(4,128)(2,1)S(1)} collective-permute-done((bf16[32,1,3,2048]{3,2,1,0:T(4,128)(2,1)S(1)}, bf16[32,1,3,2048]{3,2,1,0:T(4,128)(2,1)S(1)}, u32[]{:S(2)}, u32[]{:S(2)}) %collective-permute-start.5) | collective-permute-done | bytes 393248 | tf_op jit(solution)/shard_map/ppermute | solution.py:29
  69.1 2.8 collective-permute-start.7
  72.6 5.1 %collective-permute-done.7 = bf16[32,1,3,2048]{3,2,1,0:T(4,128)(2,1)S(1)} collective-permute-done((bf16[32,1,3,2048]{3,2,1,0:T(4,128)(2,1)S(1)}, bf16[32,1,3,2048]{3,2,1,0:T(4,128)(2,1)S(1)}, u32[]{:S(2)}, u32[]{:S(2)}) %collective-permute-start.7) | collective-permute-done | bytes 393248 | tf_op jit(solution)/shard_map/ppermute | solution.py:29
  77.7 4.1 %collective-permute-start.9 = (bf16[32,1,3,2048]{3,2,1,0:T(4,128)(2,1)S(1)}, bf16[32,1,3,2048]{3,2,1,0:T(4,128)(2,1)S(1)}, u32[]{:S(2)}, u32[]{:S(2)}) collective-permute-start(bf16[32,1,3,2048]{3,2,1,0:T(4,128)(2,1)S(1)} %collective-permute-done.7), channel_id=1, source_target_pairs={{0,1},{1,2},{2,3},{3,4},{4,5},{5,6},{6,7},{7,8},{8,9},{9,10},{10,1... | collective-permute-start | bytes 1179656 | tf_op jit(solution)/shard_map/ppermute | solution.py:29
  82.5 3.9 %collective-permute-done.9 = bf16[32,1,3,2048]{3,2,1,0:T(4,128)(2,1)S(1)} collective-permute-done((bf16[32,1,3,2048]{3,2,1,0:T(4,128)(2,1)S(1)}, bf16[32,1,3,2048]{3,2,1,0:T(4,128)(2,1)S(1)}, u32[]{:S(2)}, u32[]{:S(2)}) %collective-permute-start.9) | collective-permute-done | bytes 393248 | tf_op jit(solution)/shard_map/ppermute | solution.py:29
  86.3 5.3 %collective-permute-start.11 = (bf16[32,1,3,2048]{3,2,1,0:T(4,128)(2,1)S(1)}, bf16[32,1,3,2048]{3,2,1,0:T(4,128)(2,1)S(1)}, u32[]{:S(2)}, u32[]{:S(2)}) collective-permute-start(bf16[32,1,3,2048]{3,2,1,0:T(4,128)(2,1)S(1)} %collective-permute-done.9), channel_id=1, source_target_pairs={{0,1},{1,2},{2,3},{3,4},{4,5},{5,6},{6,7},{7,8},{8,9},{9,10},{10,1... | collective-permute-start | bytes 1179656 | tf_op jit(solution)/shard_map/ppermute | solution.py:29
  92.3 2.6 collective-permute-done.11
  94.9 6.5 %collective-permute-start.13 = (bf16[32,1,3,2048]{3,2,1,0:T(4,128)(2,1)S(1)}, bf16[32,1,3,2048]{3,2,1,0:T(4,128)(2,1)S(1)}, u32[]{:S(2)}, u32[]{:S(2)}) collective-permute-start(bf16[32,1,3,2048]{3,2,1,0:T(4,128)(2,1)S(1)} %collective-permute-done.11), channel_id=1, source_target_pairs={{0,1},{1,2},{2,3},{3,4},{4,5},{5,6},{6,7},{7,8},{8,9},{9,10},{10,1... | collective-permute-start | bytes 1179656 | tf_op jit(solution)/shard_map/ppermute | solution.py:29
  102.1 1.5 collective-permute-done.13
  103.5 7.7 %collective-permute-start.15 = (bf16[32,1,3,2048]{3,2,1,0:T(4,128)(2,1)S(1)}, bf16[32,1,3,2048]{3,2,1,0:T(4,128)(2,1)S(1)}, u32[]{:S(2)}, u32[]{:S(2)}) collective-permute-start(bf16[32,1,3,2048]{3,2,1,0:T(4,128)(2,1)S(1)} %collective-permute-done.13), channel_id=1, source_target_pairs={{0,1},{1,2},{2,3},{3,4},{4,5},{5,6},{6,7},{7,8},{8,9},{9,10},{10,1... | collective-permute-start | bytes 1179656 | tf_op jit(solution)/shard_map/ppermute | solution.py:29
  113.1 2.6 copy-done.1
  115.7 1.8 fusion.4
  117.6 12.1 %convert_bitcast_fusion = bf16[512,1,3,2048]{3,0,2,1:T(8,128)(2,1)} fusion(bf16[1,128,2048]{2,1,0:T(8,128)(2,1)S(1)} %copy-done.4, bf16[512,3,2048]{2,0,1:T(8,128)(2,1)} %copy-done.1, bf16[1,2048,128]{2,1,0:T(8,128)(2,1)S(1)} %copy-done.5, f32[512,1,3,128]{3,0,2,1:T(8,128)S(1)} %fusion.4), kind=kOutput, calls=%fused_computation | convolution fusion | flops 1615527936 | bytes 14417920 | tf_op jit(solution)/shard_map/aecf,efd->aecd/dot_general | solution.py:182
  129.7 11.4 %copy.63 = bf16[512,1,3,2048]{3,2,0,1:T(4,128)(2,1)} copy(bf16[512,1,3,2048]{3,0,2,1:T(8,128)(2,1)} %convert_bitcast_fusion) | data formatting | bytes 12582912 | tf_op jit(solution)/shard_map/convert_element_type | solution.py:184
  141.1 16.3 %reshape.301 = bf16[16,96,2048]{2,1,0:T(8,128)(2,1)} reshape(bf16[512,1,3,2048]{3,2,0,1:T(4,128)(2,1)} %copy.63) | data formatting | bytes 12582912 | tf_op jit(solution)/shard_map/reshape | solution.py:185
  157.4 16.5 %all-to-all-start.1 = ((bf16[16,96,2048]{2,1,0:T(8,128)(2,1)}), bf16[16,96,2048]{2,1,0:T(8,128)(2,1)}, u32[]{:S(2)}, u32[]{:S(2)}) async-start(bf16[16,96,2048]{2,1,0:T(8,128)(2,1)} %reshape.301), calls=%async_computation.2 | async-start | bytes 12582912 | tf_op jit(solution)/shard_map/all_to_all | solution.py:186
  174.2 2.8 collective-permute-start
  180.1 2.1 convolution_convert_fusion
  182.2 141.0 %all-to-all-done.1 = bf16[16,96,2048]{2,1,0:T(8,128)(2,1)} async-done(((bf16[16,96,2048]{2,1,0:T(8,128)(2,1)}), bf16[16,96,2048]{2,1,0:T(8,128)(2,1)}, u32[]{:S(2)}, u32[]{:S(2)}) %all-to-all-start.1) | async-done | bytes 6291488 | tf_op jit(solution)/shard_map/all_to_all | solution.py:186
  323.2 4.1 %reduce_sum.76 = bf16[96,2048]{1,0:T(8,128)(2,1)S(1)} reduce(bf16[16,96,2048]{2,1,0:T(8,128)(2,1)} %all-to-all-done.1, bf16[]{:T(256)} %constant.147.clone.1), dimensions={0}, to_apply=%region_10.11 | reduce | flops 2949120 | bytes 6684674 | tf_op jit(solution)/shard_map/reduce_sum | solution.py:187
  328.3 4.6 %all-to-all-start.2 = ((bf16[32,3,2048]{2,1,0:T(4,128)(2,1)}), bf16[32,3,2048]{2,1,0:T(4,128)(2,1)S(1)}, u32[]{:S(2)}, u32[]{:S(2)}) async-start(bf16[32,3,2048]{2,1,0:T(4,128)(2,1)} %reshape.302), calls=%async_computation.3 | async-start | bytes 1048576 | tf_op jit(solution)/shard_map/all_to_all | solution.py:189
  333.5 17.5 %all-to-all-done.2 = bf16[32,3,2048]{2,1,0:T(4,128)(2,1)S(1)} async-done(((bf16[32,3,2048]{2,1,0:T(4,128)(2,1)}), bf16[32,3,2048]{2,1,0:T(4,128)(2,1)S(1)}, u32[]{:S(2)}, u32[]{:S(2)}) %all-to-all-start.2) | async-done | bytes 393248 | tf_op jit(solution)/shard_map/all_to_all | solution.py:189
  351.0 1.1 fusion.1
  (102 shorter events, 14.8 us)
Async XLA Ops:
  7.2 172.9 %copy-start = (bf16[192,2048]{1,0:T(8,128)(2,1)S(1)}, bf16[192,2048]{1,0:T(8,128)(2,1)}, u32[]{:S(2)}) copy-start(bf16[192,2048]{1,0:T(8,128)(2,1)} %param.20) | copy-start | bytes 2359300
  12.4 30.9 %all-to-all-start = ((bf16[32,1,3,2048]{3,2,1,0:T(4,128)(2,1)}), bf16[32,1,3,2048]{3,2,1,0:T(4,128)(2,1)S(1)}, u32[]{:S(2)}, u32[]{:S(2)}) async-start(bf16[32,1,3,2048]{3,2,1,0:T(4,128)(2,1)} %copy.46), calls=%async_computation.1 | async-start | bytes 1048576 | tf_op jit(solution)/shard_map/all_to_all | solution.py:180
  43.3 8.6 %collective-permute-start.1 = (bf16[32,1,3,2048]{3,2,1,0:T(4,128)(2,1)S(1)}, bf16[32,1,3,2048]{3,2,1,0:T(4,128)(2,1)S(1)}, u32[]{:S(2)}, u32[]{:S(2)}) collective-permute-start(bf16[32,1,3,2048]{3,2,1,0:T(4,128)(2,1)S(1)} %all-to-all-done), channel_id=1, source_target_pairs={{0,1},{1,2},{2,3},{3,4},{4,5},{5,6},{6,7},{7,8},{8,9},{9,10},{10,1... | collective-permute-start | bytes 1179656 | tf_op jit(solution)/shard_map/ppermute | solution.py:29
  43.3 9.3 %collective-permute-start.2 = (bf16[32,1,3,2048]{3,2,1,0:T(4,128)(2,1)S(1)}, bf16[32,1,3,2048]{3,2,1,0:T(4,128)(2,1)S(1)}, u32[]{:S(2)}, u32[]{:S(2)}) collective-permute-start(bf16[32,1,3,2048]{3,2,1,0:T(4,128)(2,1)S(1)} %all-to-all-done), channel_id=1, source_target_pairs={{0,15},{1,0},{2,1},{3,2},{4,3},{5,4},{6,5},{7,6},{8,7},{9,8},{10,9... | collective-permute-start | bytes 1179656 | tf_op jit(solution)/shard_map/ppermute | solution.py:34
  51.9 8.6 %collective-permute-start.3 = (bf16[32,1,3,2048]{3,2,1,0:T(4,128)(2,1)S(1)}, bf16[32,1,3,2048]{3,2,1,0:T(4,128)(2,1)S(1)}, u32[]{:S(2)}, u32[]{:S(2)}) collective-permute-start(bf16[32,1,3,2048]{3,2,1,0:T(4,128)(2,1)S(1)} %collective-permute-done.1), channel_id=1, source_target_pairs={{0,1},{1,2},{2,3},{3,4},{4,5},{5,6},{6,7},{7,8},{8,9},{9,10},{10,1... | collective-permute-start | bytes 1179656 | tf_op jit(solution)/shard_map/ppermute | solution.py:29
  52.7 9.8 %collective-permute-start.4 = (bf16[32,1,3,2048]{3,2,1,0:T(4,128)(2,1)S(1)}, bf16[32,1,3,2048]{3,2,1,0:T(4,128)(2,1)S(1)}, u32[]{:S(2)}, u32[]{:S(2)}) collective-permute-start(bf16[32,1,3,2048]{3,2,1,0:T(4,128)(2,1)S(1)} %collective-permute-done.2), channel_id=1, source_target_pairs={{0,15},{1,0},{2,1},{3,2},{4,3},{5,4},{6,5},{7,6},{8,7},{9,8},{10,9... | collective-permute-start | bytes 1179656 | tf_op jit(solution)/shard_map/ppermute | solution.py:34
  54.0 61.8 %copy-start.10 = (bf16[1,2048,128]{2,1,0:T(8,128)(2,1)S(1)}, bf16[1,2048,128]{2,1,0:T(8,128)(2,1)}, u32[]{:S(2)}) copy-start(bf16[1,2048,128]{2,1,0:T(8,128)(2,1)} %param.25) | copy-start | bytes 1572868
  60.5 8.6 %collective-permute-start.5 = (bf16[32,1,3,2048]{3,2,1,0:T(4,128)(2,1)S(1)}, bf16[32,1,3,2048]{3,2,1,0:T(4,128)(2,1)S(1)}, u32[]{:S(2)}, u32[]{:S(2)}) collective-permute-start(bf16[32,1,3,2048]{3,2,1,0:T(4,128)(2,1)S(1)} %collective-permute-done.3), channel_id=1, source_target_pairs={{0,1},{1,2},{2,3},{3,4},{4,5},{5,6},{6,7},{7,8},{8,9},{9,10},{10,1... | collective-permute-start | bytes 1179656 | tf_op jit(solution)/shard_map/ppermute | solution.py:29
  62.5 9.8 %collective-permute-start.6 = (bf16[32,1,3,2048]{3,2,1,0:T(4,128)(2,1)S(1)}, bf16[32,1,3,2048]{3,2,1,0:T(4,128)(2,1)S(1)}, u32[]{:S(2)}, u32[]{:S(2)}) collective-permute-start(bf16[32,1,3,2048]{3,2,1,0:T(4,128)(2,1)S(1)} %collective-permute-done.4), channel_id=1, source_target_pairs={{0,15},{1,0},{2,1},{3,2},{4,3},{5,4},{6,5},{7,6},{8,7},{9,8},{10,9... | collective-permute-start | bytes 1179656 | tf_op jit(solution)/shard_map/ppermute | solution.py:34
  69.1 8.6 %collective-permute-start.7 = (bf16[32,1,3,2048]{3,2,1,0:T(4,128)(2,1)S(1)}, bf16[32,1,3,2048]{3,2,1,0:T(4,128)(2,1)S(1)}, u32[]{:S(2)}, u32[]{:S(2)}) collective-permute-start(bf16[32,1,3,2048]{3,2,1,0:T(4,128)(2,1)S(1)} %collective-permute-done.5), channel_id=1, source_target_pairs={{0,1},{1,2},{2,3},{3,4},{4,5},{5,6},{6,7},{7,8},{8,9},{9,10},{10,1... | collective-permute-start | bytes 1179656 | tf_op jit(solution)/shard_map/ppermute | solution.py:29
  72.3 9.8 %collective-permute-start.8 = (bf16[32,1,3,2048]{3,2,1,0:T(4,128)(2,1)S(1)}, bf16[32,1,3,2048]{3,2,1,0:T(4,128)(2,1)S(1)}, u32[]{:S(2)}, u32[]{:S(2)}) collective-permute-start(bf16[32,1,3,2048]{3,2,1,0:T(4,128)(2,1)S(1)} %collective-permute-done.6), channel_id=1, source_target_pairs={{0,15},{1,0},{2,1},{3,2},{4,3},{5,4},{6,5},{7,6},{8,7},{9,8},{10,9... | collective-permute-start | bytes 1179656 | tf_op jit(solution)/shard_map/ppermute | solution.py:34
  77.7 8.6 %collective-permute-start.9 = (bf16[32,1,3,2048]{3,2,1,0:T(4,128)(2,1)S(1)}, bf16[32,1,3,2048]{3,2,1,0:T(4,128)(2,1)S(1)}, u32[]{:S(2)}, u32[]{:S(2)}) collective-permute-start(bf16[32,1,3,2048]{3,2,1,0:T(4,128)(2,1)S(1)} %collective-permute-done.7), channel_id=1, source_target_pairs={{0,1},{1,2},{2,3},{3,4},{4,5},{5,6},{6,7},{7,8},{8,9},{9,10},{10,1... | collective-permute-start | bytes 1179656 | tf_op jit(solution)/shard_map/ppermute | solution.py:29
  82.1 9.8 %collective-permute-start.10 = (bf16[32,1,3,2048]{3,2,1,0:T(4,128)(2,1)S(1)}, bf16[32,1,3,2048]{3,2,1,0:T(4,128)(2,1)S(1)}, u32[]{:S(2)}, u32[]{:S(2)}) collective-permute-start(bf16[32,1,3,2048]{3,2,1,0:T(4,128)(2,1)S(1)} %collective-permute-done.8), channel_id=1, source_target_pairs={{0,15},{1,0},{2,1},{3,2},{4,3},{5,4},{6,5},{7,6},{8,7},{9,8},{10,9... | collective-permute-start | bytes 1179656 | tf_op jit(solution)/shard_map/ppermute | solution.py:34
  86.3 8.6 %collective-permute-start.11 = (bf16[32,1,3,2048]{3,2,1,0:T(4,128)(2,1)S(1)}, bf16[32,1,3,2048]{3,2,1,0:T(4,128)(2,1)S(1)}, u32[]{:S(2)}, u32[]{:S(2)}) collective-permute-start(bf16[32,1,3,2048]{3,2,1,0:T(4,128)(2,1)S(1)} %collective-permute-done.9), channel_id=1, source_target_pairs={{0,1},{1,2},{2,3},{3,4},{4,5},{5,6},{6,7},{7,8},{8,9},{9,10},{10,1... | collective-permute-start | bytes 1179656 | tf_op jit(solution)/shard_map/ppermute | solution.py:29
  91.9 9.8 %collective-permute-start.12 = (bf16[32,1,3,2048]{3,2,1,0:T(4,128)(2,1)S(1)}, bf16[32,1,3,2048]{3,2,1,0:T(4,128)(2,1)S(1)}, u32[]{:S(2)}, u32[]{:S(2)}) collective-permute-start(bf16[32,1,3,2048]{3,2,1,0:T(4,128)(2,1)S(1)} %collective-permute-done.10), channel_id=1, source_target_pairs={{0,15},{1,0},{2,1},{3,2},{4,3},{5,4},{6,5},{7,6},{8,7},{9,8},{10,9... | collective-permute-start | bytes 1179656 | tf_op jit(solution)/shard_map/ppermute | solution.py:34
  92.3 25.3 %copy-start.4 = (bf16[1,128,2048]{2,1,0:T(8,128)(2,1)S(1)}, bf16[1,128,2048]{2,1,0:T(8,128)(2,1)}, u32[]{:S(2)}) copy-start(bf16[1,128,2048]{2,1,0:T(8,128)(2,1)} %param.27) | copy-start | bytes 1572868
  92.3 25.3 %copy-start.5 = (bf16[1,2048,128]{2,1,0:T(8,128)(2,1)S(1)}, bf16[1,2048,128]{2,1,0:T(8,128)(2,1)}, u32[]{:S(2)}) copy-start(bf16[1,2048,128]{2,1,0:T(8,128)(2,1)} %param.26) | copy-start | bytes 1572868
  94.9 8.6 %collective-permute-start.13 = (bf16[32,1,3,2048]{3,2,1,0:T(4,128)(2,1)S(1)}, bf16[32,1,3,2048]{3,2,1,0:T(4,128)(2,1)S(1)}, u32[]{:S(2)}, u32[]{:S(2)}) collective-permute-start(bf16[32,1,3,2048]{3,2,1,0:T(4,128)(2,1)S(1)} %collective-permute-done.11), channel_id=1, source_target_pairs={{0,1},{1,2},{2,3},{3,4},{4,5},{5,6},{6,7},{7,8},{8,9},{9,10},{10,1... | collective-permute-start | bytes 1179656 | tf_op jit(solution)/shard_map/ppermute | solution.py:29
  101.7 9.8 %collective-permute-start.14 = (bf16[32,1,3,2048]{3,2,1,0:T(4,128)(2,1)S(1)}, bf16[32,1,3,2048]{3,2,1,0:T(4,128)(2,1)S(1)}, u32[]{:S(2)}, u32[]{:S(2)}) collective-permute-start(bf16[32,1,3,2048]{3,2,1,0:T(4,128)(2,1)S(1)} %collective-permute-done.12), channel_id=1, source_target_pairs={{0,15},{1,0},{2,1},{3,2},{4,3},{5,4},{6,5},{7,6},{8,7},{9,8},{10,9... | collective-permute-start | bytes 1179656 | tf_op jit(solution)/shard_map/ppermute | solution.py:34
  103.5 9.2 %collective-permute-start.15 = (bf16[32,1,3,2048]{3,2,1,0:T(4,128)(2,1)S(1)}, bf16[32,1,3,2048]{3,2,1,0:T(4,128)(2,1)S(1)}, u32[]{:S(2)}, u32[]{:S(2)}) collective-permute-start(bf16[32,1,3,2048]{3,2,1,0:T(4,128)(2,1)S(1)} %collective-permute-done.13), channel_id=1, source_target_pairs={{0,1},{1,2},{2,3},{3,4},{4,5},{5,6},{6,7},{7,8},{8,9},{9,10},{10,1... | collective-permute-start | bytes 1179656 | tf_op jit(solution)/shard_map/ppermute | solution.py:29
  113.1 2.7 copy-start.1
  157.4 16.6 %copy-start.3 = (bf16[512,64]{0,1:T(8,128)(2,1)S(1)}, bf16[512,64]{0,1:T(8,128)(2,1)}, u32[]{:S(2)}) copy-start(bf16[512,64]{0,1:T(8,128)(2,1)} %param.15) | copy-start | bytes 196612
  157.4 16.7 %copy-start.8 = (f32[1,64]{1,0:T(1,128)S(1)}, f32[1,64]{1,0:T(1,128)}, u32[]{:S(2)}) copy-start(f32[1,64]{1,0:T(1,128)} %param.18) | copy-start | bytes 772
  157.4 16.8 %copy-start.6 = (bf16[512,64]{0,1:T(8,128)(2,1)S(1)}, bf16[512,64]{0,1:T(8,128)(2,1)}, u32[]{:S(2)}) copy-start(bf16[512,64]{0,1:T(8,128)(2,1)} %param.16) | copy-start | bytes 196612
  157.4 19.6 %copy-start.2 = (bf16[512,192]{0,1:T(8,128)(2,1)S(1)}, bf16[512,192]{0,1:T(8,128)(2,1)}, u32[]{:S(2)}) copy-start(bf16[512,192]{0,1:T(8,128)(2,1)} %param.14) | copy-start | bytes 589828
  157.4 21.2 %copy-start.11 = (f32[3,64]{1,0:T(4,128)S(1)}, f32[3,64]{1,0:T(4,128)}, u32[]{:S(2)}) copy-start(f32[3,64]{1,0:T(4,128)} %param.17) | copy-start | bytes 2308
  157.4 21.7 %copy-start.9 = (f32[3]{0:T(128)S(1)}, f32[3]{0:T(128)}, u32[]{:S(2)}) copy-start(f32[3]{0:T(128)} %param.19) | copy-start | bytes 40
  157.4 165.8 %all-to-all-start.1 = ((bf16[16,96,2048]{2,1,0:T(8,128)(2,1)}), bf16[16,96,2048]{2,1,0:T(8,128)(2,1)}, u32[]{:S(2)}, u32[]{:S(2)}) async-start(bf16[16,96,2048]{2,1,0:T(8,128)(2,1)} %reshape.301), calls=%async_computation.2 | async-start | bytes 12582912 | tf_op jit(solution)/shard_map/all_to_all | solution.py:186
  174.0 178.1 %reduce-scatter.2.cloned.1.call-start = ((), (), s32[]{:S(2)}) async-start(), calls=%async_computation.4 | async-start | bytes 2228224 | tf_op jit(solution)/shard_map/reduce_scatter | solution.py:155
  174.2 4.4 %collective-permute-start = (bf16[2,128,1,64]{1,3,2,0:T(8,128)(2,1)S(1)}, bf16[2,128,1,64]{1,3,2,0:T(8,128)(2,1)S(1)}, u32[]{:S(2)}, u32[]{:S(2)}) collective-permute-start(bf16[2,128,1,64]{1,3,2,0:T(8,128)(2,1)S(1)} %pad_maximum_fusion.2), channel_id=1, source_target_pairs={{0,16},{16,32},{32,48},{48,64},{64,80},{80,96},{96,112},{112,128},... | collective-permute-start | bytes 98312 | tf_op jit(solution)/shard_map/ppermute | solution.py:48
  180.1 152.9 %copy-start.7 = (f32[32,2]{0,1:T(2,128)S(1)}, f32[32,2]{0,1:T(2,128)}, u32[]{:S(2)}) copy-start(f32[32,2]{0,1:T(2,128)} %param.24) | copy-start | bytes 772
  328.3 22.7 %all-to-all-start.2 = ((bf16[32,3,2048]{2,1,0:T(4,128)(2,1)}), bf16[32,3,2048]{2,1,0:T(4,128)(2,1)S(1)}, u32[]{:S(2)}, u32[]{:S(2)}) async-start(bf16[32,3,2048]{2,1,0:T(4,128)(2,1)} %reshape.302), calls=%async_computation.3 | async-start | bytes 1048576 | tf_op jit(solution)/shard_map/all_to_all | solution.py:189
Sparse Core Ops, SparseCore 0:
  182.3 132.2 reduce-scatter.1
